TPU v7x, 32 devices: a whole 2x2x4 slice. The times are simulated.
32 devices in a mesh: fs: 8 (over z, x), tp: 4 (over y, core).
Axes of the slice: x: 2, y: 2, z: 4, core: 2. Of those that a mesh axis runs over, the one named last changes fastest.
Arguments:
- tokens: bfloat16 [8192, 2048], P('fs', 'tp'), may hold values from -6 to 6
- recurrence_norm_gain: float32 [2048], replicated, may hold values from 0.1 to 1.9
- output_gate_weight: bfloat16 [2048, 2816], P('fs', 'tp'), may hold values from -0.125 to 0.125
- recurrence_input_weight: bfloat16 [2048, 2816], P('fs', 'tp'), may hold values from -0.125 to 0.125
- convolution_taps: float32 [4, 2816], P(None, 'tp'), may hold values from -3 to 3
- recurrence_gate_weight: bfloat16 [8, 352, 352], P('tp'), may hold values from -0.3125 to 0.3125
- input_gate_weight: bfloat16 [8, 352, 352], P('tp'), may hold values from -0.3125 to 0.3125
- base_decay_logit: float32 [2816], P('tp'), may hold values from 4.5 to 9.5
- token_log_decay: float32 [8192], P('fs'), may hold values from -0.7 to 0, as said below
- recurrence_output_weight: bfloat16 [2816, 2048], P('tp', 'fs'), may hold values from -0.4375 to 0.4375
- feedforward_norm_gain: float32 [2048], replicated, may hold values from 0.1 to 1.9
- feedforward_gate_weight: bfloat16 [2048, 5632], P('fs', 'tp'), may hold values from -0.125 to 0.125
- feedforward_up_weight: bfloat16 [2048, 5632], P('fs', 'tp'), may hold values from -0.125 to 0.125
- feedforward_down_weight: bfloat16 [5632, 2048], P('tp', 'fs'), may hold values from -0.15625 to 0.15625
Outputs:
- layer_out: bfloat16 [8192, 2048], P('fs', 'tp')
Inputs may be any that keep to these rules, and one draw needn't show every extreme that they name: `token_log_decay`: each entry is zero or lies between -0.7 and -0.22.
All inputs are finite; a program needn't handle non-finite values.
Results may differ from a plain program's by a relative error of at most 0.022.
Values may be sent and summed in bfloat16 or wider, within the bound.
A program may use at most 128 MiB of HBM per device.

v0:
```python
import functools

import jax
import jax.numpy as jnp
from jax import lax
from jax.experimental import pallas as pl
from jax.experimental.pallas import tpu as pltpu
from jax.sharding import PartitionSpec as P


LEN = 128
EPSILON = 1e-06
GATE_EXPONENT = 8.0


def ring_order(count):
    return tuple(range(0, count, 2)) + tuple(range(count - 1, 0, -2))


def ring_tables(count):
    order = ring_order(count)
    place = [0] * count
    for spot, index in enumerate(order):
        place[index] = spot
    shifts = [0]
    for step in range(1, count // 2):
        shifts += [-step, step]
    shifts.append(count // 2)
    table = [[order[(place[index] + shift) % count] for shift in shifts] for index in range(count)]
    return jnp.array(table, jnp.int32)[lax.axis_index("fs")]


def ring_gather(piece, count):
    order = ring_order(count)
    right = [(order[i], order[(i + 1) % count]) for i in range(count)]
    left = [(order[i], order[(i - 1) % count]) for i in range(count)]

    def hop(value, pairs):
        return lax.ppermute(value, "fs", pairs)

    found = [piece]
    forward = backward = piece
    half = count // 2
    for _ in range(1, half):
        forward = hop(forward, right)
        backward = hop(backward, left)
        found += [forward, backward]
    cut = piece.shape[0] // 2
    found.append(hop(forward[:cut], right))
    found.append(hop(backward[cut:], left))
    return found


def collect(owners_ref, pieces, whole_ref):
    rows = pieces[0].shape[1]
    for k, piece in enumerate(pieces[:-2]):
        spot = pl.ds(pl.multiple_of(owners_ref[k] * rows, rows), rows)
        for lead in range(2):
            whole_ref[lead, spot, :] = piece[lead]
    spot = pl.ds(pl.multiple_of(owners_ref[len(pieces) - 2] * rows, rows), rows)
    for lead in range(2):
        whole_ref[lead, spot, :] = pieces[len(pieces) - 2 + lead][0]


def norm_block(values_ref, gain_ref):
    widened = values_ref[...].astype(jnp.float32)
    scaled = widened * lax.rsqrt(jnp.mean(widened * widened, axis=-1, keepdims=True) + EPSILON)
    return (scaled * gain_ref[...]).astype(jnp.bfloat16)


ROWS = 2 * LEN
ORDERED = pltpu.CompilerParams(dimension_semantics=("arbitrary",), vmem_limit_bytes=60 * 1024 * 1024)


def once(shape):
    zeros = (0,) * len(shape)
    return pl.BlockSpec(shape, lambda i, *_: zeros, pipeline_mode=pl.Buffered(1))


def block_dense(weight):
    groups, block_width, _ = weight.shape
    identity = jnp.eye(groups, dtype=jnp.bfloat16)[:, None, :, None]
    return (weight[:, :, None, :] * identity).reshape(groups * block_width, groups * block_width)


def shift_down(values, amount, place, fill):
    return jnp.where(place >= amount, pltpu.roll(values, amount, 0), fill)


def mixer_kernel(owners_ref, rows_ref, gain_ref, taps_ref, recur_ref, inject_ref, rate_ref, token_ref, *rest):
    pieces, (out_ref, whole_ref) = rest[:-2], rest[-2:]

    @pl.when(pl.program_id(0) == 0)
    def _():
        collect(owners_ref, pieces, whole_ref)

    normed = norm_block(rows_ref, gain_ref)
    feature = jnp.dot(normed, whole_ref[1], preferred_element_type=jnp.float32)
    feature = feature.astype(jnp.bfloat16).astype(jnp.float32)
    place = lax.rem(lax.broadcasted_iota(jnp.int32, feature.shape, 0), LEN)
    taps = taps_ref[...]
    tap_count = taps.shape[0]
    summed = None
    for k in range(tap_count):
        amount = tap_count - 1 - k
        moved = shift_down(feature, amount, place, 0.0) if amount else feature
        term = taps[k : k + 1] * moved
        summed = term if summed is None else summed + term
    mixed = summed.astype(jnp.bfloat16)
    recur = jax.nn.sigmoid(jnp.dot(mixed, recur_ref[...], preferred_element_type=jnp.float32))
    inject = jax.nn.sigmoid(jnp.dot(mixed, inject_ref[...], preferred_element_type=jnp.float32))
    log_decay = rate_ref[...] * recur + token_ref[...]
    decay = jnp.exp(log_decay)
    y = 2.0 * log_decay
    series = -y * (
        1.0 + y * (1 / 2) * (1.0 + y * (1 / 3) * (1.0 + y * (1 / 4) * (1.0 + y * (1 / 5) * (1.0 + y * (1 / 6)))))
    )
    loss = jnp.where(y > -0.25, series, 1.0 - decay * decay)
    state = jnp.sqrt(loss) * (inject * mixed.astype(jnp.float32))
    amount = 1
    while amount < LEN:
        state = state + decay * shift_down(state, amount, place, 0.0)
        if 2 * amount < LEN:
            decay = decay * shift_down(decay, amount, place, 1.0)
        amount *= 2
    gate = jnp.dot(normed, whole_ref[0], preferred_element_type=jnp.float32)
    out_ref[...] = (state * jax.nn.gelu(gate)).astype(jnp.bfloat16)


def mixer(owners, full_rows, gain, taps, recur_weight, inject_weight, base_decay_logit, token_log_decay, pieces):
    rows, width = full_rows.shape
    channels = pieces[0].shape[-1]
    rate = -GATE_EXPONENT * jax.nn.softplus(-base_decay_logit)[None, :]
    block = lambda cols: pl.BlockSpec((ROWS, cols), lambda i, *_: (i, 0))
    return pl.pallas_call(
        mixer_kernel,
        grid_spec=pltpu.PrefetchScalarGridSpec(
            num_scalar_prefetch=1,
            grid=(rows // ROWS,),
            in_specs=[
                block(width),
                once((1, width)),
                once(taps.shape),
                once((channels, channels)),
                once((channels, channels)),
                once((1, channels)),
                block(1),
            ]
            + [once(piece.shape) for piece in pieces],
            out_specs=block(channels),
            scratch_shapes=[pltpu.VMEM((2, width, channels), jnp.bfloat16)],
        ),
        out_shape=jax.ShapeDtypeStruct((rows, channels), jnp.bfloat16),
        compiler_params=ORDERED,
        cost_estimate=pl.CostEstimate(
            flops=4 * rows * channels * (channels + width), bytes_accessed=4 * width * channels, transcendentals=0
        ),
    )(
        owners,
        full_rows,
        gain[None],
        taps,
        block_dense(recur_weight),
        block_dense(inject_weight),
        rate,
        token_log_decay[:, None],
        *pieces,
    )


def hidden_kernel(owners_ref, rows_ref, gain_ref, *rest):
    pieces, (out_ref, whole_ref) = rest[:-2], rest[-2:]

    @pl.when(pl.program_id(0) == 0)
    def _():
        collect(owners_ref, pieces, whole_ref)

    normed = norm_block(rows_ref, gain_ref)
    gate = jnp.dot(normed, whole_ref[0], preferred_element_type=jnp.float32)
    up = jnp.dot(normed, whole_ref[1], preferred_element_type=jnp.float32)
    out_ref[...] = (jax.nn.silu(gate) * up).astype(jnp.bfloat16)


def hidden_units(owners, full_rows, gain, pieces):
    rows, width = full_rows.shape
    units = pieces[0].shape[-1]
    block = lambda cols: pl.BlockSpec((ROWS, cols), lambda i, *_: (i, 0))
    return pl.pallas_call(
        hidden_kernel,
        grid_spec=pltpu.PrefetchScalarGridSpec(
            num_scalar_prefetch=1,
            grid=(rows // ROWS,),
            in_specs=[block(width), once((1, width))] + [once(piece.shape) for piece in pieces],
            out_specs=block(units),
            scratch_shapes=[pltpu.VMEM((2, width, units), jnp.bfloat16)],
        ),
        out_shape=jax.ShapeDtypeStruct((rows, units), jnp.bfloat16),
        compiler_params=ORDERED,
        cost_estimate=pl.CostEstimate(
            flops=4 * rows * units * width, bytes_accessed=4 * width * units, transcendentals=0
        ),
    )(owners, full_rows, gain[None], *pieces)


def down_kernel(groups, where_ref, values_ref, *rest):
    pieces, (mine_ref, other_ref) = rest[:-2], rest[-2:]
    values = values_ref[...]
    cols = pieces[0].shape[1]
    width = mine_ref.shape[2]
    y, core = where_ref[len(pieces)], where_ref[len(pieces) + 1]
    for k, piece in enumerate(pieces):
        term = jnp.dot(values, piece[...], preferred_element_type=jnp.float32).astype(jnp.bfloat16)
        start = where_ref[k] * cols
        target = start // width
        offset = pl.multiple_of(lax.rem(start, width), cols)
        turn = lax.rem(target // 2 - y + groups, groups)
        same = lax.rem(target, 2) == core

        @pl.when(same)
        def _():
            mine_ref[turn, :, pl.ds(offset, cols)] = term

        @pl.when(jnp.logical_not(same))
        def _():
            other_ref[turn, :, pl.ds(offset, cols)] = term


def project_down(owners, values, pieces, tp):
    rows, depth = values.shape
    cols = pieces[0].shape[1]
    width = cols * len(pieces) // tp
    groups = tp // 2
    tall = min(rows, 2 * ROWS)
    index = lax.axis_index("tp")
    where = jnp.concatenate([owners, jnp.stack([index // 2, index % 2]).astype(jnp.int32)])
    out_spec = pl.BlockSpec((groups, tall, width), lambda i, *_: (0, i, 0))
    shape = jax.ShapeDtypeStruct((groups, rows, width), jnp.bfloat16)
    return pl.pallas_call(
        functools.partial(down_kernel, groups),
        grid_spec=pltpu.PrefetchScalarGridSpec(
            num_scalar_prefetch=1,
            grid=(rows // tall,),
            in_specs=[pl.BlockSpec((tall, depth), lambda i, *_: (i, 0))] + [once(piece.shape) for piece in pieces],
            out_specs=[out_spec, out_spec],
        ),
        out_shape=[shape, shape],
        compiler_params=ORDERED,
        cost_estimate=pl.CostEstimate(
            flops=2 * rows * depth * cols * len(pieces), bytes_accessed=2 * depth * cols * len(pieces), transcendentals=0
        ),
    )(where, values, *pieces)


def scatter_sum(mine, other, tp):
    groups = tp // 2
    got = lax.ppermute(other, "tp", [(i, i ^ 1) for i in range(tp)])
    widen = lambda value: value.astype(jnp.float32)
    total = None
    for turn in range(1, groups):
        pair = (widen(mine[turn]) + widen(got[turn])).astype(jnp.bfloat16)
        perm = [(i, (i + 2 * turn) % tp) for i in range(tp)]
        arrived = widen(lax.ppermute(pair, "tp", perm))
        total = arrived if total is None else total + arrived
    own = widen(mine[0]) + widen(got[0])
    return own if total is None else own + total


def join_last(pieces):
    return pieces[:-2] + [jnp.concatenate(pieces[-2:], axis=0)]


def shards_general(
    count,
    tp,
    tokens,
    recurrence_norm_gain,
    output_gate_weight,
    recurrence_input_weight,
    convolution_taps,
    recurrence_gate_weight,
    input_gate_weight,
    base_decay_logit,
    token_log_decay,
    recurrence_output_weight,
    feedforward_norm_gain,
    feedforward_gate_weight,
    feedforward_up_weight,
    feedforward_down_weight,
):
    owners = ring_tables(count)
    first = ring_gather(jnp.stack([output_gate_weight, recurrence_input_weight]), count)
    out_pieces = join_last(ring_gather(recurrence_output_weight, count))
    second = ring_gather(jnp.stack([feedforward_gate_weight, feedforward_up_weight]), count)
    down_pieces = join_last(ring_gather(feedforward_down_weight, count))

    full_rows = lax.all_gather(tokens, "tp", axis=1, tiled=True)
    carried = mixer(
        owners,
        full_rows,
        recurrence_norm_gain,
        convolution_taps,
        recurrence_gate_weight,
        input_gate_weight,
        base_decay_logit,
        token_log_decay,
        first,
    )
    mine, other = project_down(owners, carried, out_pieces, tp)
    own_sum = scatter_sum(mine, other, tp)
    residual_own = (tokens.astype(jnp.float32) + own_sum).astype(jnp.bfloat16)
    residual_full = lax.all_gather(residual_own, "tp", axis=1, tiled=True)
    hidden = hidden_units(owners, residual_full, feedforward_norm_gain, second)
    chunks = 2 if hidden.shape[0] % (2 * ROWS) == 0 else 1
    size = hidden.shape[0] // chunks
    sums = []
    for chunk in range(chunks):
        mine, other = project_down(owners, hidden[chunk * size : (chunk + 1) * size], down_pieces, tp)
        sums.append(scatter_sum(mine, other, tp))
    own_down = jnp.concatenate(sums, axis=0)
    return (residual_own.astype(jnp.float32) + own_down).astype(jnp.bfloat16)


LANES = 128


def pad_lanes(values, width):
    return jnp.pad(values, [(0, 0)] * (values.ndim - 1) + [(0, width - values.shape[-1])])


def recurrence_block(prod, wide, taps, recur_w, inject_w, rate, token_col):
    gate = prod[:, :wide]
    feature = prod[:, wide:].astype(jnp.bfloat16).astype(jnp.float32)
    place = lax.rem(lax.broadcasted_iota(jnp.int32, feature.shape, 0), LEN)
    tap_count = taps.shape[0]
    summed = None
    for k in range(tap_count):
        amount = tap_count - 1 - k
        moved = shift_down(feature, amount, place, 0.0) if amount else feature
        term = taps[k : k + 1] * moved
        summed = term if summed is None else summed + term
    mixed = summed.astype(jnp.bfloat16)
    recur = jax.nn.sigmoid(jnp.dot(mixed, recur_w, preferred_element_type=jnp.float32))
    inject = jax.nn.sigmoid(jnp.dot(mixed, inject_w, preferred_element_type=jnp.float32))
    log_decay = rate * recur + token_col
    decay = jnp.exp(log_decay)
    y = 2.0 * log_decay
    series = -y * (
        1.0 + y * (1 / 2) * (1.0 + y * (1 / 3) * (1.0 + y * (1 / 4) * (1.0 + y * (1 / 5) * (1.0 + y * (1 / 6)))))
    )
    loss = jnp.where(y > -0.25, series, 1.0 - decay * decay)
    state = jnp.sqrt(loss) * (inject * mixed.astype(jnp.float32))
    amount = 1
    while amount < LEN:
        state = state + decay * shift_down(state, amount, place, 0.0)
        if 2 * amount < LEN:
            decay = decay * shift_down(decay, amount, place, 1.0)
        amount *= 2
    return (state * jax.nn.gelu(gate)).astype(jnp.bfloat16)


def layer_kernel(
    planes,
    tokens_ref,
    token_ref,
    first_ref,
    out_w_ref,
    second_ref,
    down_ref,
    gain_ref,
    gain_two_ref,
    taps_ref,
    recur_ref,
    inject_ref,
    rate_ref,
    result_ref,
    rows_ref,
    resid_ref,
    wf_ref,
    wo_ref,
    wg_ref,
    wd_ref,
    hid_ref,
    keep_ref,
    csend_ref,
    crecv_ref,
    xrecv_ref,
    ysend_ref,
    yrecv_ref,
    tokd_ref,
    local_sem,
    token_sem,
    wx_sem,
    wz_sem,
    wr_sem,
    ags_sem,
    agr_sem,
    cs_sem,
    cr_sem,
    xs_sem,
    xr_sem,
    ys_sem,
    yr_sem,
):
    fs, tp = lax.axis_index("fs"), lax.axis_index("tp")
    z, x = fs // 2, lax.rem(fs, 2)
    yy, c = tp // 2, lax.rem(tp, 2)
    ox, oy, oc = 1 - x, 1 - yy, 1 - c
    to_x, to_y, to_c = (z * 2 + ox, tp), (fs, oy * 2 + c), (fs, yy * 2 + oc)
    to_z = ((fs + 2, tp), (fs - 2, tp))
    last = planes - 1
    held, cols = tokens_ref.shape
    depth_rows = first_ref.shape[1]
    wide = wf_ref.shape[1] // 2
    chans = wo_ref.shape[0]
    units = wd_ref.shape[0]
    chunks = held // ROWS

    def mo(value, step):
        return pl.multiple_of(value, step)

    def remote(src, dst, send, recv, dest):
        return pltpu.make_async_remote_copy(
            src_ref=src, dst_ref=dst, send_sem=send, recv_sem=recv, device_id=dest, device_id_type=pl.DeviceIdType.MESH
        )

    sources = (first_ref, out_w_ref, second_ref, down_ref)

    def block(g, s):
        spot = pl.ds(mo(s * depth_rows, depth_rows), depth_rows)
        if g == 0:
            return wf_ref.at[spot, :]
        if g == 1:
            return wo_ref.at[:, spot]
        if g == 2:
            return wg_ref.at[spot, :]
        return wd_ref.at[:, spot]

    def z_copy(g, s, way, src=None):
        dst = block(g, s)
        return remote(dst if src is None else src, dst, wz_sem.at[way, g, s], wr_sem.at[g, s], to_z[way])

    def x_copy(g):
        return remote(sources[g].at[ox], block(g, fs), wx_sem.at[g], wr_sem.at[g, fs], to_x)

    def local_copy(g):
        return pltpu.make_async_copy(sources[g].at[x], block(g, fs), local_sem.at[g])

    def z_send(g, s, src=None):
        @pl.when(z < last)
        def _():
            z_copy(g, s, 0, src).start()

        @pl.when(z > 0)
        def _():
            z_copy(g, s, 1, src).start()

    def x_forward(g):
        s = z * 2 + ox
        z_copy(g, s, 0).wait_recv()
        z_send(g, s)

    def z_step(g, d):
        for side in (x, ox):

            @pl.when(z - d >= 0)
            def _():
                s = (z - d) * 2 + side
                z_copy(g, s, 0).wait_recv()

                @pl.when(z < last)
                def _():
                    z_copy(g, s, 0).start()

            @pl.when(z + d <= last)
            def _():
                s = (z + d) * 2 + side
                z_copy(g, s, 1).wait_recv()

                @pl.when(z > 0)
                def _():
                    z_copy(g, s, 1).start()

    def z_drain(g):
        x_copy(g).wait_send()
        for way in range(2):

            @pl.loop(0, 2 * planes)
            def _(s):
                sent = (s // 2 <= z) & (z < last) if way == 0 else (s // 2 >= z) & (z > 0)

                @pl.when(sent)
                def _():
                    z_copy(g, s, way).wait_send()

    def spread(buf, phase, k, slot, at, dest):
        xi, yi, ci = at
        where = buf.at[
            pl.ds(mo(xi * held + k * ROWS, ROWS), ROWS), pl.ds(mo((yi * 2 + ci) * cols, cols), cols)
        ]
        return remote(
            where, where, ags_sem.at[phase, k, slot], agr_sem.at[phase, k, xi * 4 + yi * 2 + ci], dest
        )

    own = (x, yy, c)

    def spread_own(buf, phase, k):
        spread(buf, phase, k, 0, own, to_x).start()
        spread(buf, phase, k, 1, own, to_y).start()
        spread(buf, phase, k, 2, own, to_c).start()

    def spread_x(buf, phase, k):
        at = (ox, yy, c)
        spread(buf, phase, k, 3, at, to_y).wait_recv()
        spread(buf, phase, k, 3, at, to_y).start()
        spread(buf, phase, k, 4, at, to_c).start()

    def spread_y(buf, phase, k):
        for slot, at in ((5, (x, oy, c)), (6, (ox, oy, c))):
            spread(buf, phase, k, slot, at, to_c).wait_recv()
            spread(buf, phase, k, slot, at, to_c).start()

    def spread_c(buf, phase, k):
        for xi in (x, ox):
            for yi in (yy, oy):
                spread(buf, phase, k, 2, (xi, yi, oc), to_c).wait_recv()

    def spread_drain(buf, phase, k):
        at_x = (ox, yy, c)
        spread(buf, phase, k, 0, own, to_x).wait_send()
        spread(buf, phase, k, 1, own, to_y).wait_send()
        spread(buf, phase, k, 2, own, to_c).wait_send()
        spread(buf, phase, k, 3, at_x, to_y).wait_send()
        spread(buf, phase, k, 4, at_x, to_c).wait_send()
        spread(buf, phase, k, 5, (x, oy, c), to_c).wait_send()
        spread(buf, phase, k, 6, (ox, oy, c), to_c).wait_send()

    def c_copy(j):
        return remote(csend_ref.at[j], crecv_ref.at[j], cs_sem.at[j], cr_sem.at[j], to_c)

    def x_sum_copy(j):
        return remote(keep_ref.at[j], xrecv_ref.at[j], xs_sem.at[j], xr_sem.at[j], to_x)

    def y_sum_copy(k):
        return remote(ysend_ref.at[k], yrecv_ref.at[k], ys_sem.at[k], yr_sem.at[k], to_y)

    def chunk_rows(j):
        side = jnp.where(j < chunks, ox, x)
        k = lax.rem(j, chunks)
        return side, k, pl.ds(mo(side * held + k * ROWS, ROWS), ROWS)

    def produce(j, left, weight_ref):
        for half in range(2):
            spot = pl.ds(mo((half * 2 + oc) * cols, cols), cols)
            part = jnp.dot(left, weight_ref[:, spot], preferred_element_type=jnp.float32)
            csend_ref[j, :, half * cols : (half + 1) * cols] = part.astype(jnp.bfloat16)
        for half in range(2):
            spot = pl.ds(mo((half * 2 + c) * cols, cols), cols)
            part = jnp.dot(left, weight_ref[:, spot], preferred_element_type=jnp.float32)
            keep_ref[j, :, half * cols : (half + 1) * cols] = part.astype(jnp.bfloat16)
        c_copy(j).start()

    def join_cores(j):
        c_copy(j).wait_recv()
        keep_ref[j] = (keep_ref[j].astype(jnp.float32) + crecv_ref[j].astype(jnp.float32)).astype(jnp.bfloat16)

        @pl.when(j < chunks)
        def _():
            x_sum_copy(j).start()

    def produce_all(make, weight_ref):
        @pl.loop(0, 2 * chunks)
        def _(j):
            produce(j, make(j), weight_ref)

            @pl.when(j > 0)
            def _():
                join_cores(j - 1)

        join_cores(2 * chunks - 1)

    def halves(k, side):
        spot = pl.ds(mo(side * cols, cols), cols)
        return keep_ref[chunks + k, :, spot].astype(jnp.float32) + xrecv_ref[k, :, spot].astype(jnp.float32)

    def join_x(k):
        x_sum_copy(k).wait_recv()
        ysend_ref[k] = halves(k, oy).astype(jnp.bfloat16)
        y_sum_copy(k).start()

    def join_y(k):
        y_sum_copy(k).wait_recv()
        return halves(k, yy) + yrecv_ref[k].astype(jnp.float32)

    def sums_drain():
        for j in range(2 * chunks):
            c_copy(j).wait_send()
        for k in range(chunks):
            x_sum_copy(k).wait_send()
            y_sum_copy(k).wait_send()

    own_cols = pl.ds(mo(tp * cols, cols), cols)

    def own_spot(k):
        return pl.ds(mo(x * held + k * ROWS, ROWS), ROWS)

    barrier = pltpu.get_barrier_semaphore()
    for dest in (to_x, to_y, to_c):
        pl.semaphore_signal(barrier, inc=1, device_id=dest, device_id_type=pl.DeviceIdType.MESH)

    @pl.when(z < last)
    def _():
        pl.semaphore_signal(barrier, inc=1, device_id=to_z[0], device_id_type=pl.DeviceIdType.MESH)

    @pl.when(z > 0)
    def _():
        pl.semaphore_signal(barrier, inc=1, device_id=to_z[1], device_id_type=pl.DeviceIdType.MESH)

    own_tokens = pltpu.make_async_copy(
        tokens_ref, rows_ref.at[pl.ds(mo(x * held, held), held), own_cols], token_sem.at[0]
    )
    own_decay = pltpu.make_async_copy(token_ref, tokd_ref.at[x], token_sem.at[1])
    sent_decay = remote(token_ref, tokd_ref.at[x], token_sem.at[2], token_sem.at[3], to_x)
    own_tokens.start()
    own_decay.start()
    for g in range(4):
        local_copy(g).start()
    pl.semaphore_wait(barrier, 3 + (z < last).astype(jnp.int32) + (z > 0).astype(jnp.int32))

    x_copy(0).start()
    z_send(0, fs, sources[0].at[x])
    sent_decay.start()
    own_tokens.wait()
    for k in range(chunks):
        spread_own(rows_ref, 0, k)
        if k == 0:
            x_copy(1).start()
    x_copy(2).start()
    x_copy(3).start()
    x_forward(0)
    z_step(0, 1)
    z_send(1, fs, sources[1].at[x])
    x_forward(1)
    for k in range(chunks):
        spread_x(rows_ref, 0, k)
    z_step(0, 2)
    z_step(1, 1)
    z_step(1, 2)
    z_send(2, fs, sources[2].at[x])
    for k in range(chunks):
        spread_y(rows_ref, 0, k)
    x_forward(2)
    for k in range(chunks):
        spread_c(rows_ref, 0, k)
    for g in range(4):
        local_copy(g).wait()
    own_decay.wait()
    sent_decay.wait()
    z_step(0, 3)
    z_step(1, 3)

    def mix(j):
        side, k, rows = chunk_rows(j)
        normed = norm_block(rows_ref.at[rows, :], gain_ref)
        prod = jnp.dot(normed, wf_ref[...], preferred_element_type=jnp.float32)
        columns = []
        for n in range(ROWS // LEN):
            line = tokd_ref[side, pl.ds(k * (ROWS // LEN) + n, 1), :]
            columns.append(jnp.transpose(jnp.broadcast_to(line, (LEN, LANES))))
        column = jnp.concatenate(columns, axis=0)
        column = jnp.concatenate([column] * (wide // LANES), axis=1)
        carried = recurrence_block(
            prod, wide, taps_ref[...], recur_ref[...], inject_ref[...], rate_ref[...], column
        )
        return carried[:, :chans]

    produce_all(mix, wo_ref)

    def residual_chunk(k):
        total = join_y(k) + rows_ref[own_spot(k), own_cols].astype(jnp.float32)
        resid_ref[own_spot(k), own_cols] = total.astype(jnp.bfloat16)
        spread_own(resid_ref, 1, k)

    join_x(0)
    z_step(2, 1)
    join_x(1)
    residual_chunk(0)
    join_x(2)
    residual_chunk(1)
    spread_x(resid_ref, 1, 0)
    join_x(3)
    residual_chunk(2)
    spread_x(resid_ref, 1, 1)
    residual_chunk(3)
    z_step(2, 2)
    z_send(3, fs, sources[3].at[x])
    x_forward(3)
    for k in range(2, chunks):
        spread_x(resid_ref, 1, k)
    for k in range(chunks):
        spread_y(resid_ref, 1, k)
    for k in range(chunks):
        spread_c(resid_ref, 1, k)
    sums_drain()
    z_step(2, 3)

    @pl.loop(0, 2 * chunks)
    def _(j):
        rows = pl.ds(mo(j * ROWS, ROWS), ROWS)
        normed = norm_block(resid_ref.at[rows, :], gain_two_ref)
        both = jnp.dot(normed, wg_ref[...], preferred_element_type=jnp.float32)
        hid_ref[rows, :] = (jax.nn.silu(both[:, :units]) * both[:, units:]).astype(jnp.bfloat16)

    z_step(3, 1)
    z_step(3, 2)
    z_step(3, 3)

    def lower(j):
        _, _, rows = chunk_rows(j)
        return hid_ref[rows, :]

    produce_all(lower, wd_ref)

    def result_chunk(k):
        total = join_y(k) + resid_ref[own_spot(k), own_cols].astype(jnp.float32)
        result_ref[k * ROWS : (k + 1) * ROWS, :] = total.astype(jnp.bfloat16)

    join_x(0)
    for k in range(1, chunks):
        join_x(k)
        result_chunk(k - 1)
    result_chunk(chunks - 1)

    sums_drain()
    for g in range(4):
        z_drain(g)
    for phase, buf in enumerate((rows_ref, resid_ref)):
        for k in range(chunks):
            spread_drain(buf, phase, k)


def shards_fused(
    count,
    tp,
    tokens,
    recurrence_norm_gain,
    output_gate_weight,
    recurrence_input_weight,
    convolution_taps,
    recurrence_gate_weight,
    input_gate_weight,
    base_decay_logit,
    token_log_decay,
    recurrence_output_weight,
    feedforward_norm_gain,
    feedforward_gate_weight,
    feedforward_up_weight,
    feedforward_down_weight,
):
    planes = count // 2
    x = lax.rem(lax.axis_index("fs"), 2)
    held, cols = tokens.shape
    width = cols * tp
    chans = output_gate_weight.shape[1] // 2
    units = feedforward_gate_weight.shape[1] // 2
    wide = -(-chans // LANES) * LANES
    chunks = held // ROWS

    def split(weight):
        return jnp.stack(jnp.split(weight, 2, axis=1))

    first = jnp.concatenate(
        [pad_lanes(split(output_gate_weight), wide), pad_lanes(split(recurrence_input_weight), wide)], axis=-1
    )
    second = jnp.concatenate([split(feedforward_gate_weight), split(feedforward_up_weight)], axis=-1)
    out_w = recurrence_output_weight.reshape(2, chans, -1)
    down = feedforward_down_weight.reshape(2, units, -1)
    half = lambda values, axis: lax.dynamic_slice_in_dim(values, x * chans, chans, axis)
    square = lambda weight: jnp.pad(weight[x], ((0, wide - chans), (0, wide - chans)))
    rate = -GATE_EXPONENT * jax.nn.softplus(-half(base_decay_logit, 0))[None, :]
    anywhere = pl.BlockSpec(memory_space=pl.ANY)
    inside = pl.BlockSpec(memory_space=pltpu.VMEM)
    bf16 = jnp.bfloat16
    copies = pltpu.SemaphoreType.DMA
    flops = 2 * 2 * held * (width * (2 * chans + 2 * units) + width * (chans + units))
    return pl.pallas_call(
        functools.partial(layer_kernel, planes),
        in_specs=[anywhere] * 6 + [inside] * 6,
        out_specs=inside,
        out_shape=jax.ShapeDtypeStruct((held, cols), bf16),
        scratch_shapes=[
            pltpu.VMEM((2 * held, width), bf16),
            pltpu.VMEM((2 * held, width), bf16),
            pltpu.VMEM((width, 2 * wide), bf16),
            pltpu.VMEM((chans, width), bf16),
            pltpu.VMEM((width, 2 * units), bf16),
            pltpu.VMEM((units, width), bf16),
            pltpu.VMEM((2 * held, units), bf16),
            pltpu.VMEM((2 * chunks, ROWS, 2 * cols), bf16),
            pltpu.VMEM((2 * chunks, ROWS, 2 * cols), bf16),
            pltpu.VMEM((2 * chunks, ROWS, 2 * cols), bf16),
            pltpu.VMEM((chunks, ROWS, 2 * cols), bf16),
            pltpu.VMEM((chunks, ROWS, cols), bf16),
            pltpu.VMEM((chunks, ROWS, cols), bf16),
            pltpu.VMEM((2, held // LEN, LEN), jnp.float32),
            copies((4,)),
            copies((4,)),
            copies((4,)),
            copies((2, 4, 2 * planes)),
            copies((4, 2 * planes)),
            copies((2, chunks, 7)),
            copies((2, chunks, 8)),
            copies((2 * chunks,)),
            copies((2 * chunks,)),
            copies((chunks,)),
            copies((chunks,)),
            copies((chunks,)),
            copies((chunks,)),
        ],
        compiler_params=pltpu.CompilerParams(
            collective_id=0, has_side_effects=True, vmem_limit_bytes=63 * 1024 * 1024
        ),
        cost_estimate=pl.CostEstimate(flops=flops, bytes_accessed=8 * held * width, transcendentals=0),
    )(
        tokens,
        token_log_decay.reshape(held // LEN, LEN),
        first,
        out_w,
        second,
        down,
        recurrence_norm_gain[None],
        feedforward_norm_gain[None],
        pad_lanes(half(convolution_taps, 1), wide),
        square(recurrence_gate_weight),
        square(input_gate_weight),
        pad_lanes(rate, wide),
    )


def solution(mesh):
    in_specs = (
        P("fs", "tp"),
        P(),
        P("fs", "tp"),
        P("fs", "tp"),
        P(None, "tp"),
        P("tp", None, None),
        P("tp", None, None),
        P("tp"),
        P("fs"),
        P("tp", "fs"),
        P(),
        P("fs", "tp"),
        P("fs", "tp"),
        P("tp", "fs"),
    )
    count, tp = mesh.shape["fs"], mesh.shape["tp"]
    if tp == 4:
        body = functools.partial(shards_fused, count, tp)
        return jax.shard_map(body, mesh=mesh, in_specs=in_specs, out_specs=P("fs", "tp"), check_vma=False)
    body = functools.partial(shards_general, count, tp)
    return jax.shard_map(body, mesh=mesh, in_specs=in_specs, out_specs=P("fs", "tp"), check_vma=False)
```

profile of v0, /device:TPU:7, one launch (start us, length us, event | category | flops | bytes accessed | tf_op | source)
XLA Modules:
  0.0 291.2 jit_solution(11400261181274638092)
XLA Ops:
  0.0 0.0 copy-start
  0.0 0.0 copy-start.2
  0.0 0.0 copy-start.1
  0.0 0.7 copy-done
  0.7 0.1 constant_dynamic-slice_fusion
  0.8 0.6 pad.24.taps_ref
  1.4 0.8 fusion.6
  2.2 0.6 pad.27.rate_ref
  2.8 1.1 dynamic-slice_bitcast_fusion
  3.8 0.7 pad.25.recur_ref
  4.6 0.8 pad.26.inject_ref
  5.3 0.0 copy-done.2
  5.4 0.0 copy-done.1
  5.4 0.5 slice_bitcast_fusion.1
  5.8 0.0 copy-start.3
  5.8 1.6 maximum_maximum_fusion.second_ref
  7.4 0.0 copy-done.3
  7.4 0.0 copy-start.4
  7.4 0.2 copy.19
  7.6 0.2 copy.20
  7.7 0.6 copy-done.4
  8.4 0.2 copy.21
  8.6 0.2 copy.22
  8.7 0.1 fusion.4
  8.9 0.9 pad_maximum_fusion.first_ref
  9.8 279.1 %shard_map.136 = bf16[1024,512]{1,0:T(8,128)(2,1)} custom-call(bf16[1024,512]{1,0:T(8,128)(2,1)} %tokens_ref.1, f32[8,128]{1,0:T(8,128)} %bitcast.29, bf16[2,256,768]{2,1,0:T(8,128)(2,1)} %pad_maximum_fusion.first_ref, bf16[2,352,256]{2,1,0:T(8,128)(2,1)} %bitcast.26, bf16[2,256,1408]{2,1,0:T(8,128)(2,1)} %maximum_maximum_fusion.second_ref, ...), custom_call_target="tpu_custom_call" | custom-call | flops 26575110144 | bytes 16777216 | tf_op jit(solution)/shard_map/pallas_call | solution.py:785
  288.9 2.3 copy.24
  (3 shorter events, 0.1 us)
Async XLA Ops:
  0.0 0.7 copy-start
  0.0 5.3 %copy-start.2 = (bf16[256,1408]{1,0:T(8,128)(2,1)S(1)}, bf16[256,1408]{1,0:T(8,128)(2,1)}, u32[]{:S(2)}) copy-start(bf16[256,1408]{1,0:T(8,128)(2,1)} %param.25) | copy-start | bytes 2162692
  0.0 5.3 %copy-start.1 = (bf16[256,1408]{1,0:T(8,128)(2,1)S(1)}, bf16[256,1408]{1,0:T(8,128)(2,1)}, u32[]{:S(2)}) copy-start(bf16[256,1408]{1,0:T(8,128)(2,1)} %param.26) | copy-start | bytes 2162692
  5.8 1.6 copy-start.3
  7.4 1.0 copy-start.4
where the time goes:
time: 294 us; the launch traced here: 291 us
  Pallas kernels  279 us (95%)
  local copies, waits for them, and re-layouts  8.6 us (3%)
  other arithmetic  3.4 us (1%)
    pallas_call x1, Pallas kernels, shards_fused(): pl.pallas_call(functools.partial(layer_kernel, planes), in_specs=[anywher...  279 us

commit v1 on v0

--- a/solution.py
+++ b/solution.py
@@ -327,9 +327,8 @@
     return jnp.pad(values, [(0, 0)] * (values.ndim - 1) + [(0, width - values.shape[-1])])
 
 
-def recurrence_block(prod, wide, taps, recur_w, inject_w, rate, token_col):
-    gate = prod[:, :wide]
-    feature = prod[:, wide:].astype(jnp.bfloat16).astype(jnp.float32)
+def recurrence_block(gate, feature, taps, recur_w, inject_w, rate, token_col):
+    feature = feature.astype(jnp.bfloat16).astype(jnp.float32)
     place = lax.rem(lax.broadcasted_iota(jnp.int32, feature.shape, 0), LEN)
     tap_count = taps.shape[0]
     summed = None
@@ -387,6 +386,7 @@
     ysend_ref,
     yrecv_ref,
     tokd_ref,
+    chan_ref,
     local_sem,
     token_sem,
     wx_sem,
@@ -400,6 +400,12 @@
     xr_sem,
     ys_sem,
     yr_sem,
+    dcs_sem,
+    dcr_sem,
+    dxs_sem,
+    dxr_sem,
+    dys_sem,
+    dyr_sem,
 ):
     fs, tp = lax.axis_index("fs"), lax.axis_index("tp")
     z, x = fs // 2, lax.rem(fs, 2)
@@ -459,26 +465,40 @@
         z_copy(g, s, 0).wait_recv()
         z_send(g, s)
 
-    def z_step(g, d):
-        for side in (x, ox):
-
-            @pl.when(z - d >= 0)
+    def z_pass(g, d, sides):
+        @pl.when((z > 0) & (z < last))
+        def _():
+            for side in sides:
+
+                @pl.when(z - d >= 0)
+                def _():
+                    s = (z - d) * 2 + side
+                    z_copy(g, s, 0).wait_recv()
+                    z_copy(g, s, 0).start()
+
+                @pl.when(z + d <= last)
+                def _():
+                    s = (z + d) * 2 + side
+                    z_copy(g, s, 1).wait_recv()
+                    z_copy(g, s, 1).start()
+
+    def z_end(g, d, sides):
+        for side in sides:
+
+            @pl.when((z == last) & (z - d >= 0))
             def _():
-                s = (z - d) * 2 + side
-                z_copy(g, s, 0).wait_recv()
-
-                @pl.when(z < last)
-                def _():
-                    z_copy(g, s, 0).start()
-
-            @pl.when(z + d <= last)
+                z_copy(g, (z - d) * 2 + side, 0).wait_recv()
+
+            @pl.when((z == 0) & (z + d <= last))
             def _():
-                s = (z + d) * 2 + side
-                z_copy(g, s, 1).wait_recv()
-
-                @pl.when(z > 0)
-                def _():
-                    z_copy(g, s, 1).start()
+                z_copy(g, (z + d) * 2 + side, 1).wait_recv()
+
+    def z_end_all(g):
+        for d in range(1, planes):
+            z_end(g, d, both)
+
+    both = (x, ox)
+    fixed = (0, 1)
 
     def z_drain(g):
         x_copy(g).wait_send()
@@ -508,14 +528,19 @@
         spread(buf, phase, k, 1, own, to_y).start()
         spread(buf, phase, k, 2, own, to_c).start()
 
-    def spread_x(buf, phase, k):
-        at = (ox, yy, c)
-        spread(buf, phase, k, 3, at, to_y).wait_recv()
-        spread(buf, phase, k, 3, at, to_y).start()
+    def routes(swap):
+        over_x, over_y = (ox, yy, c), (x, oy, c)
+        return (over_y, over_x, to_x) if swap else (over_x, over_y, to_y)
+
+    def spread_on(buf, phase, k, swap):
+        at, _, dest = routes(swap)
+        spread(buf, phase, k, 3, at, dest).wait_recv()
+        spread(buf, phase, k, 3, at, dest).start()
         spread(buf, phase, k, 4, at, to_c).start()
 
-    def spread_y(buf, phase, k):
-        for slot, at in ((5, (x, oy, c)), (6, (ox, oy, c))):
+    def spread_rest(buf, phase, k, swap):
+        _, other, _ = routes(swap)
+        for slot, at in ((5, other), (6, (ox, oy, c))):
             spread(buf, phase, k, slot, at, to_c).wait_recv()
             spread(buf, phase, k, slot, at, to_c).start()
 
@@ -524,24 +549,46 @@
             for yi in (yy, oy):
                 spread(buf, phase, k, 2, (xi, yi, oc), to_c).wait_recv()
 
-    def spread_drain(buf, phase, k):
-        at_x = (ox, yy, c)
+    def spread_drain(buf, phase, k, swap):
+        at, other, dest = routes(swap)
         spread(buf, phase, k, 0, own, to_x).wait_send()
         spread(buf, phase, k, 1, own, to_y).wait_send()
         spread(buf, phase, k, 2, own, to_c).wait_send()
-        spread(buf, phase, k, 3, at_x, to_y).wait_send()
-        spread(buf, phase, k, 4, at_x, to_c).wait_send()
-        spread(buf, phase, k, 5, (x, oy, c), to_c).wait_send()
+        spread(buf, phase, k, 3, at, dest).wait_send()
+        spread(buf, phase, k, 4, at, to_c).wait_send()
+        spread(buf, phase, k, 5, other, to_c).wait_send()
         spread(buf, phase, k, 6, (ox, oy, c), to_c).wait_send()
 
+    def tall(j):
+        return pl.ds(mo(j * ROWS, ROWS), ROWS)
+
     def c_copy(j):
-        return remote(csend_ref.at[j], crecv_ref.at[j], cs_sem.at[j], cr_sem.at[j], to_c)
-
-    def x_sum_copy(j):
-        return remote(keep_ref.at[j], xrecv_ref.at[j], xs_sem.at[j], xr_sem.at[j], to_x)
+        return remote(csend_ref.at[tall(j), :], crecv_ref.at[tall(j), :], cs_sem.at[j], cr_sem.at[j], to_c)
+
+    split = chunks // 2
+
+    def side_cols(side):
+        return pl.ds(mo(side * cols, cols), cols)
+
+    def x_sum_copy(k):
+        return remote(keep_ref.at[tall(k), :], xrecv_ref.at[tall(k), :], xs_sem.at[k], xr_sem.at[k], to_x)
 
     def y_sum_copy(k):
-        return remote(ysend_ref.at[k], yrecv_ref.at[k], ys_sem.at[k], yr_sem.at[k], to_y)
+        return remote(ysend_ref.at[tall(k), :], yrecv_ref.at[tall(k), :], ys_sem.at[k], yr_sem.at[k], to_y)
+
+    def y_own_copy(k):
+        src = keep_ref.at[tall(chunks + k), side_cols(oy)]
+        return remote(src, yrecv_ref.at[tall(k), :], ys_sem.at[k], yr_sem.at[k], to_y)
+
+    def y_across_copy(k):
+        src = keep_ref.at[tall(k), side_cols(oy)]
+        return remote(src, ysend_ref.at[tall(k), :], ys_sem.at[chunks + k], yr_sem.at[chunks + k], to_y)
+
+    def x_half_copy(k):
+        spot = side_cols(yy)
+        return remote(
+            keep_ref.at[tall(k), spot], xrecv_ref.at[tall(k), spot], xs_sem.at[k], xr_sem.at[k], to_x
+        )
 
     def chunk_rows(j):
         side = jnp.where(j < chunks, ox, x)
@@ -552,51 +599,190 @@
         for half in range(2):
             spot = pl.ds(mo((half * 2 + oc) * cols, cols), cols)
             part = jnp.dot(left, weight_ref[:, spot], preferred_element_type=jnp.float32)
-            csend_ref[j, :, half * cols : (half + 1) * cols] = part.astype(jnp.bfloat16)
+            csend_ref[tall(j), half * cols : (half + 1) * cols] = part.astype(jnp.bfloat16)
         for half in range(2):
             spot = pl.ds(mo((half * 2 + c) * cols, cols), cols)
             part = jnp.dot(left, weight_ref[:, spot], preferred_element_type=jnp.float32)
-            keep_ref[j, :, half * cols : (half + 1) * cols] = part.astype(jnp.bfloat16)
+            keep_ref[tall(j), half * cols : (half + 1) * cols] = part.astype(jnp.bfloat16)
         c_copy(j).start()
 
     def join_cores(j):
         c_copy(j).wait_recv()
-        keep_ref[j] = (keep_ref[j].astype(jnp.float32) + crecv_ref[j].astype(jnp.float32)).astype(jnp.bfloat16)
-
-        @pl.when(j < chunks)
+        keep_ref[tall(j), :] = (
+            keep_ref[tall(j), :].astype(jnp.float32) + crecv_ref[tall(j), :].astype(jnp.float32)
+        ).astype(jnp.bfloat16)
+
+        @pl.when(j < split)
         def _():
             x_sum_copy(j).start()
 
-    def produce_all(make, weight_ref):
+        @pl.when((j >= split) & (j < chunks))
+        def _():
+            y_across_copy(j).start()
+
+        @pl.when(j >= chunks + split)
+        def _():
+            y_own_copy(j - chunks).start()
+
+    def turn(i):
+        across = lax.rem(i, 2) * split + i // 2
+        mine = chunks + lax.rem(i - chunks + split + chunks, chunks)
+        return jnp.where(i < chunks, across, mine)
+
+    def produce_all():
         @pl.loop(0, 2 * chunks)
-        def _(j):
-            produce(j, make(j), weight_ref)
-
-            @pl.when(j > 0)
+        def _(i):
+            j = turn(i)
+            _, _, rows = chunk_rows(j)
+            produce(j, hid_ref[rows, :chans], wo_ref)
+
+            @pl.when(i > 0)
             def _():
-                join_cores(j - 1)
-
-        join_cores(2 * chunks - 1)
+                join_cores(turn(i - 1))
+
+        join_cores(turn(2 * chunks - 1))
 
     def halves(k, side):
-        spot = pl.ds(mo(side * cols, cols), cols)
-        return keep_ref[chunks + k, :, spot].astype(jnp.float32) + xrecv_ref[k, :, spot].astype(jnp.float32)
+        spot = side_cols(side)
+        return keep_ref[tall(chunks + k), spot].astype(jnp.float32) + xrecv_ref[tall(k), spot].astype(jnp.float32)
 
     def join_x(k):
         x_sum_copy(k).wait_recv()
-        ysend_ref[k] = halves(k, oy).astype(jnp.bfloat16)
+        ysend_ref[tall(k), :] = halves(k, oy).astype(jnp.bfloat16)
         y_sum_copy(k).start()
 
+    def join_across(k):
+        y_across_copy(k).wait_recv()
+        spot = side_cols(yy)
+        keep_ref[tall(k), spot] = (
+            keep_ref[tall(k), spot].astype(jnp.float32) + ysend_ref[tall(k), :].astype(jnp.float32)
+        ).astype(jnp.bfloat16)
+        x_half_copy(k).start()
+
     def join_y(k):
-        y_sum_copy(k).wait_recv()
-        return halves(k, yy) + yrecv_ref[k].astype(jnp.float32)
+        if k < split:
+            y_sum_copy(k).wait_recv()
+        else:
+            y_own_copy(k).wait_recv()
+            x_half_copy(k).wait_recv()
+        return halves(k, yy) + yrecv_ref[tall(k), :].astype(jnp.float32)
 
     def sums_drain():
         for j in range(2 * chunks):
             c_copy(j).wait_send()
         for k in range(chunks):
-            x_sum_copy(k).wait_send()
-            y_sum_copy(k).wait_send()
+            if k < split:
+                x_sum_copy(k).wait_send()
+                y_sum_copy(k).wait_send()
+            else:
+                y_own_copy(k).wait_send()
+                y_across_copy(k).wait_send()
+                x_half_copy(k).wait_send()
+
+    def near(n):
+        orders = [sorted(range(planes), key=lambda other: (abs(other - p), other)) for p in range(planes)]
+        found = orders[0][n]
+        for p in range(1, planes):
+            found = jnp.where(z == p, orders[p][n], found)
+        return found
+
+    x_rows = pl.ds(mo(ox * held, held), held)
+    own_rows = pl.ds(mo(x * held, held), held)
+
+    def wide_cols(zi, xi):
+        return pl.ds(mo((zi * 2 + xi) * depth_rows, depth_rows), depth_rows)
+
+    def slot_cols(zi, xi):
+        return pl.ds(mo((zi // 2 * 2 + xi) * depth_rows, depth_rows), depth_rows)
+
+    def down_c_copy(zi, xi, half):
+        rows = own_rows if half else x_rows
+        at = zi * 2 + xi
+        return remote(
+            rows_ref.at[rows, wide_cols(zi, xi)],
+            crecv_ref.at[rows, slot_cols(zi, xi)],
+            dcs_sem.at[half, at],
+            dcr_sem.at[half, at],
+            to_c,
+        )
+
+    def down_x_copy(zi, xi):
+        at = zi * 2 + xi
+        return remote(
+            rows_ref.at[x_rows, wide_cols(zi, xi)],
+            xrecv_ref.at[:, slot_cols(zi, xi)],
+            dxs_sem.at[at],
+            dxr_sem.at[at],
+            to_x,
+        )
+
+    def down_y_copy(zi, xi):
+        return remote(
+            rows_ref.at[own_rows, wide_cols(zi, xi)],
+            yrecv_ref.at[:, xi * depth_rows : (xi + 1) * depth_rows],
+            dys_sem.at[xi],
+            dyr_sem.at[xi],
+            to_y,
+        )
+
+    def lower(zi, xi, half):
+        rows = own_rows if half else x_rows
+        part = jnp.dot(hid_ref[rows, :], wd_ref[:, wide_cols(zi, xi)], preferred_element_type=jnp.float32)
+        rows_ref[rows, wide_cols(zi, xi)] = part.astype(jnp.bfloat16)
+
+        @pl.when(lax.rem(zi, 2) == oc)
+        def _():
+            down_c_copy(zi, xi, half).start()
+
+    def gather(zi, xi, half):
+        @pl.when(lax.rem(zi, 2) == c)
+        def _():
+            rows = own_rows if half else x_rows
+            down_c_copy(zi, xi, half).wait_recv()
+            rows_ref[rows, wide_cols(zi, xi)] = (
+                rows_ref[rows, wide_cols(zi, xi)].astype(jnp.float32)
+                + crecv_ref[rows, slot_cols(zi, xi)].astype(jnp.float32)
+            ).astype(jnp.bfloat16)
+            if half == 0:
+                down_x_copy(zi, xi).start()
+
+    def both_x(zi, xi):
+        return rows_ref[own_rows, wide_cols(zi, xi)].astype(jnp.float32) + xrecv_ref[:, slot_cols(zi, xi)].astype(
+            jnp.float32
+        )
+
+    def down_join_x(zi, xi):
+        @pl.when(lax.rem(zi, 2) == c)
+        def _():
+            down_x_copy(zi, xi).wait_recv()
+
+            @pl.when(zi // 2 == oy)
+            def _():
+                rows_ref[own_rows, wide_cols(zi, xi)] = both_x(zi, xi).astype(jnp.bfloat16)
+                down_y_copy(zi, xi).start()
+
+    def down_last(zi, xi):
+        @pl.when(zi == tp)
+        def _():
+            down_y_copy(zi, xi).wait_recv()
+            spot = slice(xi * depth_rows, (xi + 1) * depth_rows)
+            total = both_x(zi, xi) + yrecv_ref[:, spot].astype(jnp.float32)
+            total = total + resid_ref[own_rows, wide_cols(zi, xi)].astype(jnp.float32)
+            result_ref[:, spot] = total.astype(jnp.bfloat16)
+
+    def down_drain(zi, xi):
+        @pl.when(lax.rem(zi, 2) == oc)
+        def _():
+            for half in range(2):
+                down_c_copy(zi, xi, half).wait_send()
+
+        @pl.when(lax.rem(zi, 2) == c)
+        def _():
+            down_x_copy(zi, xi).wait_send()
+
+            @pl.when(zi // 2 == oy)
+            def _():
+                down_y_copy(zi, xi).wait_send()
 
     own_cols = pl.ds(mo(tp * cols, cols), cols)
 
@@ -628,6 +814,7 @@
 
     x_copy(0).start()
     z_send(0, fs, sources[0].at[x])
+    z_send(1, fs, sources[1].at[x])
     sent_decay.start()
     own_tokens.wait()
     for k in range(chunks):
@@ -636,106 +823,139 @@
             x_copy(1).start()
     x_copy(2).start()
     x_copy(3).start()
+    first_half = x == 0
+    chan_ref[0 : taps_ref.shape[0], :] = jnp.where(first_half, taps_ref[:, :chans], taps_ref[:, chans:])
+    chan_ref[taps_ref.shape[0] : taps_ref.shape[0] + 1, :] = jnp.where(
+        first_half, rate_ref[:, :chans], rate_ref[:, chans:]
+    )
     x_forward(0)
-    z_step(0, 1)
-    z_send(1, fs, sources[1].at[x])
+    z_pass(0, 1, both)
+    for k in range(chunks):
+        spread_on(rows_ref, 0, k, False)
+    z_pass(0, 2, both)
     x_forward(1)
+    z_pass(1, 1, both)
     for k in range(chunks):
-        spread_x(rows_ref, 0, k)
-    z_step(0, 2)
-    z_step(1, 1)
-    z_step(1, 2)
-    z_send(2, fs, sources[2].at[x])
-    for k in range(chunks):
-        spread_y(rows_ref, 0, k)
-    x_forward(2)
+        spread_rest(rows_ref, 0, k, False)
     for k in range(chunks):
         spread_c(rows_ref, 0, k)
     for g in range(4):
         local_copy(g).wait()
     own_decay.wait()
     sent_decay.wait()
-    z_step(0, 3)
-    z_step(1, 3)
-
-    def mix(j):
-        side, k, rows = chunk_rows(j)
-        normed = norm_block(rows_ref.at[rows, :], gain_ref)
-        prod = jnp.dot(normed, wf_ref[...], preferred_element_type=jnp.float32)
-        columns = []
-        for n in range(ROWS // LEN):
-            line = tokd_ref[side, pl.ds(k * (ROWS // LEN) + n, 1), :]
-            columns.append(jnp.transpose(jnp.broadcast_to(line, (LEN, LANES))))
-        column = jnp.concatenate(columns, axis=0)
-        column = jnp.concatenate([column] * (wide // LANES), axis=1)
-        carried = recurrence_block(
-            prod, wide, taps_ref[...], recur_ref[...], inject_ref[...], rate_ref[...], column
-        )
-        return carried[:, :chans]
-
-    produce_all(mix, wo_ref)
+    z_end_all(0)
+
+    def mix(start):
+        @pl.loop(start, start + chunks)
+        def _(j):
+            side, k, rows = chunk_rows(j)
+            normed = norm_block(rows_ref.at[rows, :], gain_ref)
+            prod = jnp.dot(normed, wf_ref[...], preferred_element_type=jnp.float32)
+            columns = []
+            for n in range(ROWS // LEN):
+                line = tokd_ref[side, pl.ds(k * (ROWS // LEN) + n, 1), :]
+                columns.append(jnp.transpose(jnp.broadcast_to(line, (LEN, LANES))))
+            column = jnp.concatenate(columns, axis=0)
+            column = jnp.concatenate([column] * (wide // LANES), axis=1)[:, :chans]
+            taps = chan_ref[0 : taps_ref.shape[0], :]
+            rate = chan_ref[taps_ref.shape[0] : taps_ref.shape[0] + 1, :]
+            hid_ref[rows, :chans] = recurrence_block(
+                prod[:, :chans], prod[:, wide : wide + chans], taps, recur_ref[x], inject_ref[x], rate, column
+            )
+
+    mix(0)
+    z_pass(1, 2, both)
+    z_send(2, fs, sources[2].at[x])
+    x_forward(2)
+    mix(chunks)
+    z_end_all(1)
+    produce_all()
 
     def residual_chunk(k):
         total = join_y(k) + rows_ref[own_spot(k), own_cols].astype(jnp.float32)
         resid_ref[own_spot(k), own_cols] = total.astype(jnp.bfloat16)
         spread_own(resid_ref, 1, k)
 
-    join_x(0)
-    z_step(2, 1)
-    join_x(1)
-    residual_chunk(0)
-    join_x(2)
-    residual_chunk(1)
-    spread_x(resid_ref, 1, 0)
-    join_x(3)
-    residual_chunk(2)
-    spread_x(resid_ref, 1, 1)
-    residual_chunk(3)
-    z_step(2, 2)
-    z_send(3, fs, sources[3].at[x])
-    x_forward(3)
-    for k in range(2, chunks):
-        spread_x(resid_ref, 1, k)
-    for k in range(chunks):
-        spread_y(resid_ref, 1, k)
+    for k in range(split, chunks):
+        join_across(k)
+    z_pass(2, 1, (x,))
+    for k in range(split):
+        join_x(k)
+    z_pass(2, 1, (ox,))
+    weave = [k + side for k in range(split) for side in (split, 0)]
+    for k in weave:
+        residual_chunk(k)
+    z_pass(2, 2, (x,))
+    for k in weave:
+        spread_on(resid_ref, 1, k, k % 2 == 1)
+    z_pass(2, 2, (ox,))
+    z_copy(3, z * 2 + ox, 0).wait_recv()
+    for xi in range(2):
+        z_send(3, z * 2 + xi)
+    for k in weave:
+        spread_rest(resid_ref, 1, k, k % 2 == 1)
     for k in range(chunks):
         spread_c(resid_ref, 1, k)
     sums_drain()
-    z_step(2, 3)
-
-    @pl.loop(0, 2 * chunks)
-    def _(j):
-        rows = pl.ds(mo(j * ROWS, ROWS), ROWS)
-        normed = norm_block(resid_ref.at[rows, :], gain_two_ref)
-        both = jnp.dot(normed, wg_ref[...], preferred_element_type=jnp.float32)
-        hid_ref[rows, :] = (jax.nn.silu(both[:, :units]) * both[:, units:]).astype(jnp.bfloat16)
-
-    z_step(3, 1)
-    z_step(3, 2)
-    z_step(3, 3)
-
-    def lower(j):
-        _, _, rows = chunk_rows(j)
-        return hid_ref[rows, :]
-
-    produce_all(lower, wd_ref)
-
-    def result_chunk(k):
-        total = join_y(k) + resid_ref[own_spot(k), own_cols].astype(jnp.float32)
-        result_ref[k * ROWS : (k + 1) * ROWS, :] = total.astype(jnp.bfloat16)
-
-    join_x(0)
-    for k in range(1, chunks):
-        join_x(k)
-        result_chunk(k - 1)
-    result_chunk(chunks - 1)
-
-    sums_drain()
+    for k in range(chunks):
+        spread_drain(rows_ref, 0, k, False)
+    z_end_all(2)
+
+    def hide(start):
+        @pl.loop(start, start + chunks)
+        def _(j):
+            _, _, rows = chunk_rows(j)
+            normed = norm_block(resid_ref.at[rows, :], gain_two_ref)
+            pair = jnp.dot(normed, wg_ref[...], preferred_element_type=jnp.float32)
+            hid_ref[rows, :] = (jax.nn.silu(pair[:, :units]) * pair[:, units:]).astype(jnp.bfloat16)
+
+    def half_sums(n, half):
+        for xi in range(2):
+            lower(near(n), xi, half)
+        for xi in range(2):
+            gather(near(n), xi, half)
+
+    def near_join(n):
+        for xi in range(2):
+            down_join_x(near(n), xi)
+
+    def near_last(n):
+        for xi in range(2):
+            down_last(near(n), xi)
+
+    hide(0)
+    half_sums(0, 0)
+    z_pass(3, 1, fixed)
+    hide(chunks)
+    half_sums(0, 1)
+    z_pass(3, 2, fixed)
+    z_end(3, 1, fixed)
+    half_sums(1, 0)
+    half_sums(1, 1)
+    near_join(0)
+    z_end(3, 2, fixed)
+    half_sums(2, 0)
+    half_sums(2, 1)
+    near_join(1)
+    for xi in range(2):
+        z_end(3, 3, (xi,))
+        lower(near(3), xi, 0)
+        lower(near(3), xi, 1)
+        gather(near(3), xi, 0)
+        gather(near(3), xi, 1)
+        if xi == 0:
+            near_join(2)
+    near_join(3)
+    for n in range(planes):
+        near_last(n)
+
+    for n in range(planes):
+        for xi in range(2):
+            down_drain(near(n), xi)
     for g in range(4):
         z_drain(g)
-    for phase, buf in enumerate((rows_ref, resid_ref)):
-        for k in range(chunks):
-            spread_drain(buf, phase, k)
+    for k in range(chunks):
+        spread_drain(resid_ref, 1, k, k % 2 == 1)
 
 
 def shards_fused(
@@ -757,7 +977,6 @@
     feedforward_down_weight,
 ):
     planes = count // 2
-    x = lax.rem(lax.axis_index("fs"), 2)
     held, cols = tokens.shape
     width = cols * tp
     chans = output_gate_weight.shape[1] // 2
@@ -774,9 +993,7 @@
     second = jnp.concatenate([split(feedforward_gate_weight), split(feedforward_up_weight)], axis=-1)
     out_w = recurrence_output_weight.reshape(2, chans, -1)
     down = feedforward_down_weight.reshape(2, units, -1)
-    half = lambda values, axis: lax.dynamic_slice_in_dim(values, x * chans, chans, axis)
-    square = lambda weight: jnp.pad(weight[x], ((0, wide - chans), (0, wide - chans)))
-    rate = -GATE_EXPONENT * jax.nn.softplus(-half(base_decay_logit, 0))[None, :]
+    rate = -GATE_EXPONENT * jax.nn.softplus(-base_decay_logit)[None, :]
     anywhere = pl.BlockSpec(memory_space=pl.ANY)
     inside = pl.BlockSpec(memory_space=pltpu.VMEM)
     bf16 = jnp.bfloat16
@@ -795,13 +1012,14 @@
             pltpu.VMEM((width, 2 * units), bf16),
             pltpu.VMEM((units, width), bf16),
             pltpu.VMEM((2 * held, units), bf16),
-            pltpu.VMEM((2 * chunks, ROWS, 2 * cols), bf16),
-            pltpu.VMEM((2 * chunks, ROWS, 2 * cols), bf16),
-            pltpu.VMEM((2 * chunks, ROWS, 2 * cols), bf16),
-            pltpu.VMEM((chunks, ROWS, 2 * cols), bf16),
-            pltpu.VMEM((chunks, ROWS, cols), bf16),
-            pltpu.VMEM((chunks, ROWS, cols), bf16),
+            pltpu.VMEM((2 * held, 2 * cols), bf16),
+            pltpu.VMEM((2 * held, 2 * cols), bf16),
+            pltpu.VMEM((2 * held, 2 * cols), bf16),
+            pltpu.VMEM((held, 2 * cols), bf16),
+            pltpu.VMEM((held, cols), bf16),
+            pltpu.VMEM((held, cols), bf16),
             pltpu.VMEM((2, held // LEN, LEN), jnp.float32),
+            pltpu.VMEM((convolution_taps.shape[0] + 1, chans), jnp.float32),
             copies((4,)),
             copies((4,)),
             copies((4,)),
@@ -813,8 +1031,14 @@
             copies((2 * chunks,)),
             copies((chunks,)),
             copies((chunks,)),
-            copies((chunks,)),
-            copies((chunks,)),
+            copies((2 * chunks,)),
+            copies((2 * chunks,)),
+            copies((2, 2 * planes)),
+            copies((2, 2 * planes)),
+            copies((2 * planes,)),
+            copies((2 * planes,)),
+            copies((2,)),
+            copies((2,)),
         ],
         compiler_params=pltpu.CompilerParams(
             collective_id=0, has_side_effects=True, vmem_limit_bytes=63 * 1024 * 1024
@@ -829,10 +1053,10 @@
         down,
         recurrence_norm_gain[None],
         feedforward_norm_gain[None],
-        pad_lanes(half(convolution_taps, 1), wide),
-        square(recurrence_gate_weight),
-        square(input_gate_weight),
-        pad_lanes(rate, wide),
+        convolution_taps,
+        recurrence_gate_weight,
+        input_gate_weight,
+        rate,
     )
 
 

time: 294 us -> 260 us (0.88)
  Pallas kernels: 279 us -> 250 us
    pallas_call x1, Pallas kernels: 279 us -> 250 us  [shards_fused(): pl.pallas_call(functools.partial(layer_kernel, planes), in_specs=[anywher...]
where the time goes in v1:
time: 260 us; the launch traced here: 259 us
  Pallas kernels  250 us (96%)
  local copies, waits for them, and re-layouts  6 us (2%)
  other arithmetic  2.64 us (1%)
    pallas_call x1, Pallas kernels, shards_fused(): pl.pallas_call(functools.partial(layer_kernel, planes), in_specs=[anywher...  250 us

profile of v1, /device:TPU:7, one launch (start us, length us, event | category | flops | bytes accessed | tf_op | source)
XLA Modules:
  0.0 258.9 jit_solution(8279068738067291162)
XLA Ops:
  0.0 1.8 slice_bitcast_fusion.1
  1.8 0.0 copy-start
  1.8 1.6 maximum_maximum_fusion.second_ref
  3.4 0.0 copy-done
  3.4 0.0 copy-start.1
  3.4 0.2 copy.19
  3.6 0.2 copy.20
  3.7 0.6 copy-done.1
  4.4 0.2 copy.21
  4.6 0.2 copy.22
  4.7 0.0 copy-start.2
  4.7 0.1 fusion.4
  4.9 0.9 pad_maximum_fusion.first_ref
  5.8 0.0 copy-done.2
  5.8 0.6 mul.10.rate_ref
  6.4 250.2 %shard_map.136 = bf16[1024,512]{1,0:T(8,128)(2,1)} custom-call(bf16[1024,512]{1,0:T(8,128)(2,1)} %tokens_ref.1, f32[8,128]{1,0:T(8,128)} %bitcast.25, bf16[2,256,768]{2,1,0:T(8,128)(2,1)} %pad_maximum_fusion.first_ref, bf16[2,352,256]{2,1,0:T(8,128)(2,1)} %bitcast.22, bf16[2,256,1408]{2,1,0:T(8,128)(2,1)} %maximum_maximum_fusion.second_ref, ...), custom_call_target="tpu_custom_call" | custom-call | flops 26575110144 | bytes 16777216 | tf_op jit(solution)/shard_map/pallas_call | solution.py:1002
  256.6 2.3 copy.24
  (3 shorter events, 0.1 us)
Async XLA Ops:
  1.8 1.6 copy-start
  3.4 1.0 copy-start.1
  4.7 1.1 copy-start.2

commit v2 on v1

--- a/solution.py
+++ b/solution.py
@@ -321,10 +321,7 @@
 
 
 LANES = 128
-
-
-def pad_lanes(values, width):
-    return jnp.pad(values, [(0, 0)] * (values.ndim - 1) + [(0, width - values.shape[-1])])
+PIECES = 2
 
 
 def recurrence_block(gate, feature, taps, recur_w, inject_w, rate, token_col):
@@ -361,9 +358,11 @@
     planes,
     tokens_ref,
     token_ref,
-    first_ref,
+    gate_in_ref,
+    feature_in_ref,
     out_w_ref,
-    second_ref,
+    gate_up_ref,
+    up_ref,
     down_ref,
     gain_ref,
     gain_two_ref,
@@ -388,6 +387,7 @@
     tokd_ref,
     chan_ref,
     local_sem,
+    raw_sem,
     token_sem,
     wx_sem,
     wz_sem,
@@ -411,12 +411,12 @@
     z, x = fs // 2, lax.rem(fs, 2)
     yy, c = tp // 2, lax.rem(tp, 2)
     ox, oy, oc = 1 - x, 1 - yy, 1 - c
+    here = (fs, tp)
     to_x, to_y, to_c = (z * 2 + ox, tp), (fs, oy * 2 + c), (fs, yy * 2 + oc)
     to_z = ((fs + 2, tp), (fs - 2, tp))
     last = planes - 1
     held, cols = tokens_ref.shape
-    depth_rows = first_ref.shape[1]
-    wide = wf_ref.shape[1] // 2
+    depth_rows = gate_in_ref.shape[2]
     chans = wo_ref.shape[0]
     units = wd_ref.shape[0]
     chunks = held // ROWS
@@ -429,12 +429,14 @@
             src_ref=src, dst_ref=dst, send_sem=send, recv_sem=recv, device_id=dest, device_id_type=pl.DeviceIdType.MESH
         )
 
-    sources = (first_ref, out_w_ref, second_ref, down_ref)
+    staged = resid_ref.at[0:depth_rows, : 2 * units]
+    raw = [resid_ref.at[n * depth_rows : (n + 1) * depth_rows, : 2 * units] for n in range(1, 3)]
+    sources = (None, out_w_ref, None, down_ref)
 
     def block(g, s):
         spot = pl.ds(mo(s * depth_rows, depth_rows), depth_rows)
         if g == 0:
-            return wf_ref.at[spot, :]
+            return wf_ref.at[:, spot]
         if g == 1:
             return wo_ref.at[:, spot]
         if g == 2:
@@ -446,7 +448,19 @@
         return remote(dst if src is None else src, dst, wz_sem.at[way, g, s], wr_sem.at[g, s], to_z[way])
 
     def x_copy(g):
-        return remote(sources[g].at[ox], block(g, fs), wx_sem.at[g], wr_sem.at[g, fs], to_x)
+        src = staged if g == 2 else sources[g].at[ox]
+        return remote(src, block(g, fs), wx_sem.at[g], wr_sem.at[g, fs], to_x)
+
+    projections = (gate_in_ref, feature_in_ref)
+
+    def first_spot(n):
+        return wf_ref.at[n * chans : (n + 1) * chans, pl.ds(mo(fs * depth_rows, depth_rows), depth_rows)]
+
+    def first_x_copy(n):
+        return remote(projections[n].at[ox], first_spot(n), wx_sem.at[4 * n], wr_sem.at[0, fs], to_x)
+
+    def first_local_copy(n):
+        return pltpu.make_async_copy(projections[n].at[x], first_spot(n), local_sem.at[2 * n])
 
     def local_copy(g):
         return pltpu.make_async_copy(sources[g].at[x], block(g, fs), local_sem.at[g])
@@ -501,7 +515,6 @@
     fixed = (0, 1)
 
     def z_drain(g):
-        x_copy(g).wait_send()
         for way in range(2):
 
             @pl.loop(0, 2 * planes)
@@ -706,22 +719,27 @@
             to_c,
         )
 
-    def down_x_copy(zi, xi):
+    piece = held // PIECES
+
+    def piece_rows(side, p):
+        return pl.ds(mo(side * held + p * piece, piece), piece)
+
+    def down_x_copy(zi, xi, p):
         at = zi * 2 + xi
         return remote(
-            rows_ref.at[x_rows, wide_cols(zi, xi)],
-            xrecv_ref.at[:, slot_cols(zi, xi)],
-            dxs_sem.at[at],
-            dxr_sem.at[at],
+            rows_ref.at[piece_rows(ox, p), wide_cols(zi, xi)],
+            xrecv_ref.at[p * piece : (p + 1) * piece, slot_cols(zi, xi)],
+            dxs_sem.at[p, at],
+            dxr_sem.at[p, at],
             to_x,
         )
 
-    def down_y_copy(zi, xi):
+    def down_y_copy(zi, xi, p):
         return remote(
-            rows_ref.at[own_rows, wide_cols(zi, xi)],
-            yrecv_ref.at[:, xi * depth_rows : (xi + 1) * depth_rows],
-            dys_sem.at[xi],
-            dyr_sem.at[xi],
+            rows_ref.at[piece_rows(x, p), wide_cols(zi, xi)],
+            yrecv_ref.at[p * piece : (p + 1) * piece, xi * depth_rows : (xi + 1) * depth_rows],
+            dys_sem.at[p, xi],
+            dyr_sem.at[p, xi],
             to_y,
         )
 
@@ -737,52 +755,57 @@
     def gather(zi, xi, half):
         @pl.when(lax.rem(zi, 2) == c)
         def _():
-            rows = own_rows if half else x_rows
             down_c_copy(zi, xi, half).wait_recv()
-            rows_ref[rows, wide_cols(zi, xi)] = (
-                rows_ref[rows, wide_cols(zi, xi)].astype(jnp.float32)
-                + crecv_ref[rows, slot_cols(zi, xi)].astype(jnp.float32)
-            ).astype(jnp.bfloat16)
-            if half == 0:
-                down_x_copy(zi, xi).start()
-
-    def both_x(zi, xi):
-        return rows_ref[own_rows, wide_cols(zi, xi)].astype(jnp.float32) + xrecv_ref[:, slot_cols(zi, xi)].astype(
-            jnp.float32
-        )
+            for p in range(PIECES):
+                rows = piece_rows(x if half else ox, p)
+                rows_ref[rows, wide_cols(zi, xi)] = (
+                    rows_ref[rows, wide_cols(zi, xi)].astype(jnp.float32)
+                    + crecv_ref[rows, slot_cols(zi, xi)].astype(jnp.float32)
+                ).astype(jnp.bfloat16)
+                if half == 0:
+                    down_x_copy(zi, xi, p).start()
+
+    def both_x(zi, xi, p):
+        mine = rows_ref[piece_rows(x, p), wide_cols(zi, xi)].astype(jnp.float32)
+        return mine + xrecv_ref[p * piece : (p + 1) * piece, slot_cols(zi, xi)].astype(jnp.float32)
 
     def down_join_x(zi, xi):
         @pl.when(lax.rem(zi, 2) == c)
         def _():
-            down_x_copy(zi, xi).wait_recv()
+            for p in range(PIECES):
+                down_x_copy(zi, xi, p).wait_recv()
+
+                @pl.when(zi // 2 == oy)
+                def _():
+                    rows_ref[piece_rows(x, p), wide_cols(zi, xi)] = both_x(zi, xi, p).astype(jnp.bfloat16)
+                    down_y_copy(zi, xi, p).start()
+
+    def down_last(zi, xi):
+        @pl.when(zi == tp)
+        def _():
+            for p in range(PIECES):
+                down_y_copy(zi, xi, p).wait_recv()
+                rows = slice(p * piece, (p + 1) * piece)
+                spot = slice(xi * depth_rows, (xi + 1) * depth_rows)
+                total = both_x(zi, xi, p) + yrecv_ref[rows, spot].astype(jnp.float32)
+                total = total + resid_ref[piece_rows(x, p), wide_cols(zi, xi)].astype(jnp.float32)
+                result_ref[rows, spot] = total.astype(jnp.bfloat16)
+
+    def down_drain(zi, xi):
+        @pl.when(lax.rem(zi, 2) == oc)
+        def _():
+            for half in range(2):
+                down_c_copy(zi, xi, half).wait_send()
+
+        @pl.when(lax.rem(zi, 2) == c)
+        def _():
+            for p in range(PIECES):
+                down_x_copy(zi, xi, p).wait_send()
 
             @pl.when(zi // 2 == oy)
             def _():
-                rows_ref[own_rows, wide_cols(zi, xi)] = both_x(zi, xi).astype(jnp.bfloat16)
-                down_y_copy(zi, xi).start()
-
-    def down_last(zi, xi):
-        @pl.when(zi == tp)
-        def _():
-            down_y_copy(zi, xi).wait_recv()
-            spot = slice(xi * depth_rows, (xi + 1) * depth_rows)
-            total = both_x(zi, xi) + yrecv_ref[:, spot].astype(jnp.float32)
-            total = total + resid_ref[own_rows, wide_cols(zi, xi)].astype(jnp.float32)
-            result_ref[:, spot] = total.astype(jnp.bfloat16)
-
-    def down_drain(zi, xi):
-        @pl.when(lax.rem(zi, 2) == oc)
-        def _():
-            for half in range(2):
-                down_c_copy(zi, xi, half).wait_send()
-
-        @pl.when(lax.rem(zi, 2) == c)
-        def _():
-            down_x_copy(zi, xi).wait_send()
-
-            @pl.when(zi // 2 == oy)
-            def _():
-                down_y_copy(zi, xi).wait_send()
+                for p in range(PIECES):
+                    down_y_copy(zi, xi, p).wait_send()
 
     own_cols = pl.ds(mo(tp * cols, cols), cols)
 
@@ -808,12 +831,29 @@
     sent_decay = remote(token_ref, tokd_ref.at[x], token_sem.at[2], token_sem.at[3], to_x)
     own_tokens.start()
     own_decay.start()
-    for g in range(4):
+    raws = [
+        pltpu.make_async_copy(source, target, raw_sem.at[n])
+        for n, (source, target) in enumerate(zip((gate_up_ref, up_ref), raw))
+    ]
+    for n in range(2):
+        first_local_copy(n).start()
+    for copy in raws:
+        copy.start()
+    for g in (1, 3):
         local_copy(g).start()
+    first_half = x == 0
+
+    def pick(values, here, width):
+        left, right = values[:, :width], values[:, width:]
+        return jnp.where(first_half == here, left, right)
+
+    for n in range(2):
+        first_local_copy(n).wait()
     pl.semaphore_wait(barrier, 3 + (z < last).astype(jnp.int32) + (z > 0).astype(jnp.int32))
 
-    x_copy(0).start()
-    z_send(0, fs, sources[0].at[x])
+    for n in range(2):
+        first_x_copy(n).start()
+    z_send(0, fs)
     z_send(1, fs, sources[1].at[x])
     sent_decay.start()
     own_tokens.wait()
@@ -821,9 +861,15 @@
         spread_own(rows_ref, 0, k)
         if k == 0:
             x_copy(1).start()
+    raws[0].wait()
+    raws[1].wait()
+    own_second = block(2, fs)
+    for n in range(2):
+        values = raw[n][...]
+        for here, target in ((True, own_second), (False, staged)):
+            target[:, n * units : (n + 1) * units] = pick(values, here, units)
     x_copy(2).start()
     x_copy(3).start()
-    first_half = x == 0
     chan_ref[0 : taps_ref.shape[0], :] = jnp.where(first_half, taps_ref[:, :chans], taps_ref[:, chans:])
     chan_ref[taps_ref.shape[0] : taps_ref.shape[0] + 1, :] = jnp.where(
         first_half, rate_ref[:, :chans], rate_ref[:, chans:]
@@ -839,7 +885,7 @@
         spread_rest(rows_ref, 0, k, False)
     for k in range(chunks):
         spread_c(rows_ref, 0, k)
-    for g in range(4):
+    for g in (1, 3):
         local_copy(g).wait()
     own_decay.wait()
     sent_decay.wait()
@@ -850,25 +896,28 @@
         def _(j):
             side, k, rows = chunk_rows(j)
             normed = norm_block(rows_ref.at[rows, :], gain_ref)
-            prod = jnp.dot(normed, wf_ref[...], preferred_element_type=jnp.float32)
+            prod = lax.dot_general(
+                normed, wf_ref[...], (((1,), (1,)), ((), ())), preferred_element_type=jnp.float32
+            )
             columns = []
             for n in range(ROWS // LEN):
                 line = tokd_ref[side, pl.ds(k * (ROWS // LEN) + n, 1), :]
                 columns.append(jnp.transpose(jnp.broadcast_to(line, (LEN, LANES))))
             column = jnp.concatenate(columns, axis=0)
-            column = jnp.concatenate([column] * (wide // LANES), axis=1)[:, :chans]
+            column = jnp.concatenate([column] * (-(-chans // LANES)), axis=1)[:, :chans]
             taps = chan_ref[0 : taps_ref.shape[0], :]
             rate = chan_ref[taps_ref.shape[0] : taps_ref.shape[0] + 1, :]
             hid_ref[rows, :chans] = recurrence_block(
-                prod[:, :chans], prod[:, wide : wide + chans], taps, recur_ref[x], inject_ref[x], rate, column
+                prod[:, :chans], prod[:, chans:], taps, recur_ref[x], inject_ref[x], rate, column
             )
 
     mix(0)
     z_pass(1, 2, both)
-    z_send(2, fs, sources[2].at[x])
+    z_send(2, fs)
     x_forward(2)
     mix(chunks)
     z_end_all(1)
+    x_copy(2).wait_send()
     produce_all()
 
     def residual_chunk(k):
@@ -889,20 +938,20 @@
     for k in weave:
         spread_on(resid_ref, 1, k, k % 2 == 1)
     z_pass(2, 2, (ox,))
-    z_copy(3, z * 2 + ox, 0).wait_recv()
-    for xi in range(2):
-        z_send(3, z * 2 + xi)
     for k in weave:
         spread_rest(resid_ref, 1, k, k % 2 == 1)
     for k in range(chunks):
         spread_c(resid_ref, 1, k)
+    z_copy(3, z * 2 + ox, 0).wait_recv()
+    for xi in range(2):
+        z_send(3, z * 2 + xi)
     sums_drain()
     for k in range(chunks):
         spread_drain(rows_ref, 0, k, False)
     z_end_all(2)
 
-    def hide(start):
-        @pl.loop(start, start + chunks)
+    def hide(start, stop):
+        @pl.loop(start, stop)
         def _(j):
             _, _, rows = chunk_rows(j)
             normed = norm_block(resid_ref.at[rows, :], gain_two_ref)
@@ -923,16 +972,17 @@
         for xi in range(2):
             down_last(near(n), xi)
 
-    hide(0)
+    hide(0, chunks)
     half_sums(0, 0)
     z_pass(3, 1, fixed)
-    hide(chunks)
-    half_sums(0, 1)
-    z_pass(3, 2, fixed)
+    hide(chunks, chunks + split)
     z_end(3, 1, fixed)
     half_sums(1, 0)
+    hide(chunks + split, 2 * chunks)
+    half_sums(0, 1)
     half_sums(1, 1)
     near_join(0)
+    z_pass(3, 2, fixed)
     z_end(3, 2, fixed)
     half_sums(2, 0)
     half_sums(2, 1)
@@ -952,6 +1002,10 @@
     for n in range(planes):
         for xi in range(2):
             down_drain(near(n), xi)
+    for n in range(2):
+        first_x_copy(n).wait_send()
+    for g in (1, 3):
+        x_copy(g).wait_send()
     for g in range(4):
         z_drain(g)
     for k in range(chunks):
@@ -981,16 +1035,8 @@
     width = cols * tp
     chans = output_gate_weight.shape[1] // 2
     units = feedforward_gate_weight.shape[1] // 2
-    wide = -(-chans // LANES) * LANES
     chunks = held // ROWS
 
-    def split(weight):
-        return jnp.stack(jnp.split(weight, 2, axis=1))
-
-    first = jnp.concatenate(
-        [pad_lanes(split(output_gate_weight), wide), pad_lanes(split(recurrence_input_weight), wide)], axis=-1
-    )
-    second = jnp.concatenate([split(feedforward_gate_weight), split(feedforward_up_weight)], axis=-1)
     out_w = recurrence_output_weight.reshape(2, chans, -1)
     down = feedforward_down_weight.reshape(2, units, -1)
     rate = -GATE_EXPONENT * jax.nn.softplus(-base_decay_logit)[None, :]
@@ -1001,13 +1047,13 @@
     flops = 2 * 2 * held * (width * (2 * chans + 2 * units) + width * (chans + units))
     return pl.pallas_call(
         functools.partial(layer_kernel, planes),
-        in_specs=[anywhere] * 6 + [inside] * 6,
+        in_specs=[anywhere] * 8 + [inside] * 6,
         out_specs=inside,
         out_shape=jax.ShapeDtypeStruct((held, cols), bf16),
         scratch_shapes=[
             pltpu.VMEM((2 * held, width), bf16),
             pltpu.VMEM((2 * held, width), bf16),
-            pltpu.VMEM((width, 2 * wide), bf16),
+            pltpu.VMEM((2 * chans, width), bf16),
             pltpu.VMEM((chans, width), bf16),
             pltpu.VMEM((width, 2 * units), bf16),
             pltpu.VMEM((units, width), bf16),
@@ -1021,8 +1067,9 @@
             pltpu.VMEM((2, held // LEN, LEN), jnp.float32),
             pltpu.VMEM((convolution_taps.shape[0] + 1, chans), jnp.float32),
             copies((4,)),
+            copies((2,)),
             copies((4,)),
-            copies((4,)),
+            copies((5,)),
             copies((2, 4, 2 * planes)),
             copies((4, 2 * planes)),
             copies((2, chunks, 7)),
@@ -1035,10 +1082,10 @@
             copies((2 * chunks,)),
             copies((2, 2 * planes)),
             copies((2, 2 * planes)),
-            copies((2 * planes,)),
-            copies((2 * planes,)),
-            copies((2,)),
-            copies((2,)),
+            copies((PIECES, 2 * planes)),
+            copies((PIECES, 2 * planes)),
+            copies((PIECES, 2)),
+            copies((PIECES, 2)),
         ],
         compiler_params=pltpu.CompilerParams(
             collective_id=0, has_side_effects=True, vmem_limit_bytes=63 * 1024 * 1024
@@ -1047,9 +1094,11 @@
     )(
         tokens,
         token_log_decay.reshape(held // LEN, LEN),
-        first,
+        output_gate_weight.T.reshape(2, chans, -1),
+        recurrence_input_weight.T.reshape(2, chans, -1),
         out_w,
-        second,
+        feedforward_gate_weight,
+        feedforward_up_weight,
         down,
         recurrence_norm_gain[None],
         feedforward_norm_gain[None],

time: 260 us -> 249 us (0.958)
  Pallas kernels: 250 us -> 243 us
  other arithmetic: 2.64 us -> 0.01 us
    pallas_call x1, Pallas kernels: 250 us -> 243 us  [shards_fused(): pl.pallas_call(functools.partial(layer_kernel, planes), in_specs=[anywher...]
where the time goes in v2:
time: 249 us; the launch traced here: 247 us
  Pallas kernels  243 us (98%)
  local copies, waits for them, and re-layouts  3.54 us (1%)
    pallas_call x1, Pallas kernels, shards_fused(): pl.pallas_call(functools.partial(layer_kernel, planes), in_specs=[anywher...  243 us

profile of v2, /device:TPU:7, one launch (start us, length us, event | category | flops | bytes accessed | tf_op | source)
XLA Modules:
  0.0 247.0 jit_solution(417235326728579153)
XLA Ops:
  0.0 0.0 copy-start
  0.0 0.7 copy-done
  0.7 0.6 mul.10.rate_ref
  1.3 243.4 %shard_map.136 = bf16[1024,512]{1,0:T(8,128)(2,1)} custom-call(bf16[1024,512]{1,0:T(8,128)(2,1)} %tokens_ref.1, f32[8,128]{1,0:T(8,128)} %bitcast.17, bf16[2,352,256]{2,1,0:T(8,128)(2,1)} %bitcast.12, bf16[2,352,256]{2,1,0:T(8,128)(2,1)} %bitcast.13, bf16[2,352,256]{2,1,0:T(8,128)(2,1)} %bitcast.14, bf16[256,1408]{1,0:T(8,128)(2,1)} %gate_up_ref.1, ...), custom_call_target="tpu_custom_call" | custom-call | flops 26575110144 | bytes 16777216 | tf_op jit(solution)/shard_map/pallas_call | solution.py:1048
  244.7 2.3 copy.16
  (1 shorter events, 0.0 us)
Async XLA Ops:
  0.0 0.7 copy-start
